TPU v7x, 32 devices: a whole 2x2x4 slice. The times are simulated.
32 devices in a mesh: sp: 8 (over z, x), tp: 4 (over y, core).
Axes of the slice: x: 2, y: 2, z: 4, core: 2. Of those that a mesh axis runs over, the one named last changes fastest.
Arguments:
- cotangent: bfloat16 [1024, 2048], P('sp'), may hold values from -6 to 6
- mixer_out: bfloat16 [1024, 2048], P('sp'), may hold values from -6 to 6
- expert_ids: int32 [1024, 2], P('sp'), may hold values from 0 to 7, all different within a row; in each aligned block of 128 rows (0 to 127, 128 to 255, ...) at most 64 rows name the same one
- route_weight: float32 [1024, 2], P('sp'), may hold values from 0.3 to 1.5
- saved_normalized: bfloat16 [1024, 2048], P('sp', 'tp'), may hold values from -6 to 6
- inverse_deviation: float32 [1024], P('sp'), may hold values from 0.3 to 3
- channel_norm_gain: float32 [2048], P('tp'), may hold values from 0.1 to 1.9
- taps: float32 [31, 2048], P(None, 'tp'), may hold values from -1 to 1
- proj_weight: bfloat16 [2048, 2048], P('tp'), may hold values from -0.125 to 0.125
- gate_weight: bfloat16 [8, 2048, 2048], P('sp', None, 'tp'), may hold values from -0.125 to 0.125
- up_weight: bfloat16 [8, 2048, 2048], P('sp', None, 'tp'), may hold values from -0.125 to 0.125
- down_weight: bfloat16 [8, 2048, 2048], P('sp', 'tp'), may hold values from -0.125 to 0.125
Outputs:
- grad_mixer_in: bfloat16 [1024, 2048], P('sp', 'tp')
- grad_proj: float32 [2048, 2048], P('sp', 'tp')
- grad_gate: bfloat16 [8, 2048, 2048], P('sp', None, 'tp')
- grad_up: bfloat16 [8, 2048, 2048], P('sp', None, 'tp')
- grad_down: bfloat16 [8, 2048, 2048], P('sp', 'tp')
Inputs may be any that keep to these rules, and one draw needn't show every extreme that they name: `expert_ids`: each row names 2 different experts. Within the rows of one index of sp no expert is named more than 64 times, a bound that some block reaches.
All inputs are finite; a program needn't handle non-finite values.
Results may differ from a plain program's by a relative error of at most 0.02.
Values may be sent and summed in bfloat16 or wider, within the bound.
A program may use at most 64 MiB of HBM per device.

v0:
```python
import jax
import jax.numpy as jnp
from jax import lax
from jax.sharding import PartitionSpec as P


def from_behind(value, axis, steps):
    count = lax.axis_size(axis)
    leading, last = (max(0, -steps), min(count, count - steps))
    return lax.ppermute(value, axis, [(source, source + steps) for source in range(leading, last)])


def route_table(expert_ids, route_weight, slot_start, slot_span, capacity, experts):
    onehot = (expert_ids[:, :, None] == jnp.arange(experts, dtype=jnp.int32)[None, None, :]).astype(
        jnp.int32
    )
    flat_hot = onehot.reshape(-1, experts)
    ranks = jnp.cumsum(flat_hot, axis=0) - flat_hot
    rank_pair = jnp.sum(ranks * flat_hot, axis=1).reshape(expert_ids.shape)
    slot_index = expert_ids * capacity + rank_pair
    targets = (
        jnp.arange(experts, dtype=jnp.int32)[:, None] * capacity
        + slot_start
        + jnp.arange(slot_span, dtype=jnp.int32)[None, :]
    ).reshape(-1)
    matched = slot_index[None, :, :] == targets[:, None, None]
    dispatch = jnp.any(matched, axis=2).astype(jnp.bfloat16)
    slot_weight = jnp.sum(jnp.where(matched, route_weight[None, :, :], 0.0), axis=(1, 2))
    return (dispatch, slot_weight)


def shards(
    cotangent,
    mixer_out,
    expert_ids,
    route_weight,
    saved_normalized,
    inverse_deviation,
    channel_norm_gain,
    taps,
    proj_weight,
    gate_weight,
    up_weight,
    down_weight,
):
    experts = lax.axis_size("sp")
    groups = lax.axis_size("tp")
    tok_rows, model_width = cotangent.shape
    capacity = groups * max(1, 4 * tok_rows // (experts * groups))
    slot_span = capacity // groups
    slot_start = lax.axis_index("tp") * slot_span
    dispatch, slot_weight = route_table(
        expert_ids, route_weight, slot_start, slot_span, capacity, experts
    )
    sent_rows = jnp.dot(dispatch, mixer_out, preferred_element_type=jnp.float32).astype(
        jnp.bfloat16
    )
    sent_grad = (
        slot_weight[:, None] * jnp.dot(dispatch, cotangent, preferred_element_type=jnp.float32)
    ).astype(jnp.bfloat16)
    sent_rows = sent_rows.reshape(experts, slot_span, model_width)
    sent_grad = sent_grad.reshape(experts, slot_span, model_width)
    shared_rows = (
        lax.all_to_all(sent_rows, "sp", split_axis=0, concat_axis=0, tiled=True),
        lax.all_to_all(sent_grad, "sp", split_axis=0, concat_axis=0, tiled=True),
    )
    routed_rows, routed_grad = (
        lax.all_gather(shared_rows[0], "tp", axis=1, tiled=True),
        lax.all_gather(shared_rows[1], "tp", axis=1, tiled=True),
    )
    full_table, unused_weight = route_table(
        expert_ids, route_weight, 0, capacity, capacity, experts
    )
    routed_rows = routed_rows.reshape(-1, model_width)
    routed_grad = routed_grad.reshape(-1, model_width)
    w_first = gate_weight[0]
    w_third = up_weight[0]
    w_second = down_weight[0]
    contract_last = (((1,), (1,)), ((), ()))
    contract_first = (((0,), (0,)), ((), ()))
    hidden_gate = jnp.dot(routed_rows, w_first, preferred_element_type=jnp.float32)
    hidden_up = jnp.dot(routed_rows, w_third, preferred_element_type=jnp.float32)
    sigma = jax.nn.sigmoid(hidden_gate)
    swish = hidden_gate * sigma
    activ = (swish * hidden_up).astype(jnp.bfloat16)
    grad_second = lax.dot_general(
        activ, routed_grad, contract_first, preferred_element_type=jnp.float32
    ).astype(jnp.bfloat16)
    grad_activ = lax.dot_general(
        routed_grad, w_second, contract_last, preferred_element_type=jnp.float32
    )
    grad_gpre = (grad_activ * hidden_up * sigma * (1.0 + hidden_gate * (1.0 - sigma))).astype(
        jnp.bfloat16
    )
    grad_upre = (grad_activ * swish).astype(jnp.bfloat16)
    grad_first = lax.dot_general(
        routed_rows, grad_gpre, contract_first, preferred_element_type=jnp.float32
    ).astype(jnp.bfloat16)
    grad_third = lax.dot_general(
        routed_rows, grad_upre, contract_first, preferred_element_type=jnp.float32
    ).astype(jnp.bfloat16)
    partial_value = lax.dot_general(
        grad_gpre, w_first, contract_last, preferred_element_type=jnp.float32
    ) + lax.dot_general(grad_upre, w_third, contract_last, preferred_element_type=jnp.float32)
    summed = lax.psum(partial_value.astype(jnp.bfloat16), "tp")
    home_rows = lax.all_to_all(
        summed.reshape(experts, capacity, model_width),
        "sp",
        split_axis=0,
        concat_axis=0,
        tiled=True,
    )
    returned = lax.dot_general(
        full_table,
        home_rows.reshape(-1, model_width),
        contract_first,
        preferred_element_type=jnp.float32,
    )
    mixer_grad = (cotangent.astype(jnp.float32) + returned).astype(jnp.bfloat16)
    normalized_input = saved_normalized.astype(jnp.float32)
    normalized_values = normalized_input * channel_norm_gain[None, :]
    gate_sig = jax.nn.sigmoid(normalized_values)
    act_conv = (normalized_values * gate_sig).astype(jnp.bfloat16)
    grad_proj = lax.psum_scatter(
        lax.dot_general(
            mixer_grad, act_conv, contract_first, preferred_element_type=jnp.float32
        ).astype(jnp.bfloat16),
        "sp",
        scatter_dimension=0,
        tiled=True,
    ).astype(jnp.float32)
    grad_act = lax.dot_general(
        mixer_grad, proj_weight, contract_last, preferred_element_type=jnp.float32
    )
    norm_output_gradient = (
        grad_act
        * gate_sig
        * (1.0 + normalized_values * (1.0 - gate_sig))
        * channel_norm_gain[None, :]
    )
    reduced_totals = lax.psum(
        (
            jnp.sum(norm_output_gradient, axis=1),
            jnp.sum(norm_output_gradient * normalized_input, axis=1),
        ),
        "tp",
    )
    channel_count = saved_normalized.shape[1] * groups
    conv_output_gradient = inverse_deviation[:, None] * (
        norm_output_gradient
        - reduced_totals[0][:, None] / channel_count
        - normalized_input * (reduced_totals[1][:, None] / channel_count)
    )
    reach = taps.shape[0] - 1
    beyond = from_behind(conv_output_gradient[:reach], "sp", -1)
    extended = jnp.concatenate([conv_output_gradient, beyond], axis=0)
    result = jnp.zeros_like(conv_output_gradient)
    for tap_index in range(taps.shape[0]):
        result = result + taps[tap_index][None, :] * extended[tap_index : tap_index + tok_rows]
    return (
        result.astype(jnp.bfloat16),
        grad_proj,
        grad_first[None],
        grad_third[None],
        grad_second[None],
    )


def solution(mesh):
    return jax.shard_map(
        shards,
        mesh=mesh,
        in_specs=(
            P("sp", None),
            P("sp", None),
            P("sp", None),
            P("sp", None),
            P("sp", "tp"),
            P("sp"),
            P("tp"),
            P(None, "tp"),
            P("tp", None),
            P("sp", None, "tp"),
            P("sp", None, "tp"),
            P("sp", "tp", None),
        ),
        out_specs=(
            P("sp", "tp"),
            P("sp", "tp"),
            P("sp", None, "tp"),
            P("sp", None, "tp"),
            P("sp", "tp", None),
        ),
        check_vma=False,
    )
```

profile of v0, /device:TPU:0, one launch (start us, length us, event | category | flops | bytes accessed | tf_op | source)
XLA Modules:
  0.0 273.1 jit_solution(8081440627756328696)
XLA Ops:
  7.3 0.9 copy.31
  8.2 0.1 eq.63
  8.3 0.1 eq.59
  8.5 0.1 iota_add_fusion
  8.6 0.1 add.181
  8.6 0.6 reduce-window.6
  9.2 0.2 slice_reduce_fusion
  9.5 0.1 fusion.124
  9.6 0.1 reshape.97
  9.7 0.1 copy.33
  9.8 0.7 multiply_add_fusion
  10.5 0.1 compare_reduce_fusion.1
  10.6 1.3 convolution_convert_fusion.4
  11.9 21.7 %all_to_all.15 = bf16[8,16,2048]{2,1,0:T(8,128)(2,1)} all-to-all(bf16[8,16,2048]{2,1,0:T(8,128)(2,1)S(1)} %bitcast.87), channel_id=1, replica_groups=mesh['sp'=8,'tp'=4] {'sp'}, dimensions={0} | all-to-all | bytes 1048576 | tf_op jit(solution)/shard_map/all_to_all | solution.py:64
  33.7 0.0 all-gather.3.cloned.1.call-start
  33.7 0.2 fusion.120
  33.9 0.3 fusion.3
  34.2 17.6 %all_to_all.16 = bf16[8,16,2048]{2,1,0:T(8,128)(2,1)} all-to-all(bf16[8,16,2048]{2,1,0:T(8,128)(2,1)S(1)} %bitcast.86), channel_id=1, replica_groups=mesh['sp'=8,'tp'=4] {'sp'}, dimensions={0} | all-to-all | bytes 1048576 | tf_op jit(solution)/shard_map/all_to_all | solution.py:65
  51.9 0.0 all-reduce.3.cloned.1.call-start
  51.9 3.5 %all-gather.5.cloned.1.call-done = bf16[8,64,2048]{2,1,0:T(8,128)(2,1)} async-done(((bf16[8,16,2048]{2,1,0:T(8,128)(2,1)}), bf16[8,64,2048]{2,1,0:T(8,128)(2,1)}) %all-gather.5.cloned.1.call-update) | async-done | bytes 2097168 | tf_op jit(solution)/shard_map/all_gather | solution.py:68
  55.4 4.0 %fusion.7 = f32[512,512]{1,0:T(8,128)} fusion(bf16[512,2048]{1,0:T(8,128)(2,1)} %bitcast.119, bf16[1,2048,512]{2,1,0:T(8,128)(2,1)S(1)} %copy-done), kind=kOutput, calls=%fused_computation.44 | convolution fusion | flops 1073741824 | bytes 5242880 | tf_op jit(solution)/shard_map/dot_general | solution.py:81
  59.4 2.3 fusion.10
  61.7 17.9 %all-gather.3.cloned.1.call-done = bf16[8,64,2048]{2,1,0:T(8,128)(2,1)} async-done(((bf16[8,16,2048]{2,1,0:T(8,128)(2,1)}), bf16[8,64,2048]{2,1,0:T(8,128)(2,1)}) %all-gather.3.cloned.1.call-update) | async-done | bytes 2097168 | tf_op jit(solution)/shard_map/all_gather | solution.py:69
  79.6 4.4 %multiply_convert_fusion.1 = (bf16[512,512]{1,0:T(8,128)(2,1)S(1)}, bf16[512,512]{1,0:T(8,128)(2,1)S(1)}) fusion(f32[512,512]{1,0:T(8,128)} %fusion.7, f32[512,512]{1,0:T(8,128)} %fusion.10, bf16[512,2048]{1,0:T(8,128)(2,1)} %bitcast.123, bf16[1,512,2048]{2,1,0:T(8,128)(2,1)} %param.23), kind=kOutput, calls=%fused_computation.55 | convolution fusion | flops 1077149696 | bytes 7340032 | tf_op jit(solution)/shard_map/dot_general | solution.py:89
  84.0 1.3 fusion.5
  85.3 0.6 copy-done.2
  85.9 2.6 add_convert_fusion
  88.6 51.5 %all-reduce.3.cloned.1.call-done = bf16[8,64,2048]{2,1,0:T(8,128)(2,1)} async-done(((bf16[8,64,2048]{2,1,0:T(8,128)(2,1)}), bf16[8,64,2048]{2,1,0:T(8,128)(2,1)}) %all-reduce.3.cloned.1.call-update) | async-done | bytes 2097168 | tf_op jit(solution)/shard_map/psum | solution.py:105
  140.1 5.5 %all-to-all-start.2 = ((bf16[8,64,2048]{2,1,0:T(8,128)(2,1)}), bf16[8,64,2048]{2,1,0:T(8,128)(2,1)}, u32[]{:S(2)}, u32[]{:S(2)}) async-start(bf16[8,64,2048]{2,1,0:T(8,128)(2,1)} %all-reduce.3.cloned.1.call-done), calls=%async_computation.2 | async-start | bytes 4194304 | tf_op jit(solution)/shard_map/all_to_all | solution.py:106
  145.7 0.1 iota_add_fusion.1
  145.8 0.1 add.175
  145.8 0.1 compare_reduce_fusion
  146.0 47.7 %all-to-all-done.2 = bf16[8,64,2048]{2,1,0:T(8,128)(2,1)} async-done(((bf16[8,64,2048]{2,1,0:T(8,128)(2,1)}), bf16[8,64,2048]{2,1,0:T(8,128)(2,1)}, u32[]{:S(2)}, u32[]{:S(2)}) %all-to-all-start.2) | async-done | bytes 2097184 | tf_op jit(solution)/shard_map/all_to_all | solution.py:106
  193.7 2.1 fusion.4
  195.8 2.1 convolution_convert_fusion
  198.0 0.6 fusion.130
  198.6 0.7 fusion.129
  199.3 4.4 %fusion.1 = bf16[1,2048,512]{2,1,0:T(8,128)(2,1)} fusion(bf16[512,2048]{1,0:T(8,128)(2,1)} %bitcast.120, bf16[512,512]{1,0:T(8,128)(2,1)S(1)} %copy-done.7), kind=kOutput, calls=%fused_computation.35 | convolution fusion | flops 1074790400 | bytes 4718592 | tf_op jit(solution)/shard_map/dot_general | solution.py:99
  203.7 2.7 fusion.2
  206.4 1.5 fusion.128
  207.9 6.2 %all-reduce = (f32[128]{0:T(128)S(1)}, f32[128]{0:T(128)S(1)}) all-reduce(f32[128]{0:T(128)} %get-tuple-element.6, f32[128]{0:T(128)} %get-tuple-element.5), channel_id=1, replica_groups=mesh['sp'=8,'tp'=4] {'tp'}, use_global_device_ids=true, to_apply=%region_10.11 | all-reduce | flops 256 | bytes 2048 | tf_op jit(solution)/shard_map/psum | solution.py:141
  214.1 0.8 fusion.27
  215.2 1.3 collective-permute-start
  216.5 4.3 %fusion = bf16[1,2048,512]{2,1,0:T(8,128)(2,1)} fusion(bf16[512,2048]{1,0:T(8,128)(2,1)} %bitcast.121, bf16[512,512]{1,0:T(8,128)(2,1)S(1)} %copy-done.5), kind=kOutput, calls=%fused_computation.34 | convolution fusion | flops 1074790400 | bytes 4718592 | tf_op jit(solution)/shard_map/dot_general | solution.py:96
  220.7 0.9 collective-permute-done
  221.9 2.0 fusion.32
  223.9 40.9 %reduce-scatter.2.cloned.1.call-done = bf16[256,512]{1,0:T(8,128)(2,1)} async-done(((bf16[2048,512]{1,0:T(8,128)(2,1)}), bf16[256,512]{1,0:T(8,128)(2,1)}) %reduce-scatter.2.cloned.1.call-update) | async-done | bytes 262160 | tf_op jit(solution)/shard_map/reduce_scatter | solution.py:124
  264.8 1.8 convert_element_type.72
  (102 shorter events, 0.4 us)
Async XLA Ops:
  7.2 48.3 %copy-start = (bf16[1,2048,512]{2,1,0:T(8,128)(2,1)S(1)}, bf16[1,2048,512]{2,1,0:T(8,128)(2,1)}, u32[]{:S(2)}) copy-start(bf16[1,2048,512]{2,1,0:T(8,128)(2,1)} %param.21) | copy-start | bytes 6291460
  7.2 26.5 %copy-start.39 = (f32[128,2]{0,1:T(2,128)S(1)}, f32[128,2]{0,1:T(2,128)}, u32[]{:S(2)}) copy-start(f32[128,2]{0,1:T(2,128)} %param.15) | copy-start | bytes 3076
  7.2 26.7 %copy-start.3 = (bf16[128,2048]{1,0:T(8,128)(2,1)S(1)}, bf16[128,2048]{1,0:T(8,128)(2,1)}, u32[]{:S(2)}) copy-start(bf16[128,2048]{1,0:T(8,128)(2,1)} %param.12) | copy-start | bytes 1572868
  7.2 48.2 %all-gather.5.cloned.1.call-start = ((), (), s32[]{:S(2)}) async-start(), calls=%async_computation.5 | async-start | bytes 2621440 | tf_op jit(solution)/shard_map/all_gather | solution.py:68
  33.7 45.9 %all-gather.3.cloned.1.call-start = ((), (), s32[]{:S(2)}) async-start(), calls=%async_computation.4 | async-start | bytes 2621440 | tf_op jit(solution)/shard_map/all_gather | solution.py:69
  51.9 88.2 %all-reduce.3.cloned.1.call-start = ((), (), s32[]{:S(2)}) async-start(), calls=%async_computation.6 | async-start | bytes 4194304 | tf_op jit(solution)/shard_map/psum | solution.py:105
  55.4 4.0 %copy-start.1 = (bf16[1,2048,512]{2,1,0:T(8,128)(2,1)S(1)}, bf16[1,2048,512]{2,1,0:T(8,128)(2,1)}, u32[]{:S(2)}) copy-start(bf16[1,2048,512]{2,1,0:T(8,128)(2,1)} %param.22) | copy-start | bytes 6291460
  55.4 4.0 %copy-start.41 = (bf16[8,64,2048]{2,1,0:T(8,128)(2,1)S(1)}, bf16[8,64,2048]{2,1,0:T(8,128)(2,1)}, u32[]{:S(2)}) copy-start(bf16[8,64,2048]{2,1,0:T(8,128)(2,1)} %all-gather.5.cloned.1.call-done) | copy-start | bytes 6291460
  140.1 53.6 %all-to-all-start.2 = ((bf16[8,64,2048]{2,1,0:T(8,128)(2,1)}), bf16[8,64,2048]{2,1,0:T(8,128)(2,1)}, u32[]{:S(2)}, u32[]{:S(2)}) async-start(bf16[8,64,2048]{2,1,0:T(8,128)(2,1)} %all-reduce.3.cloned.1.call-done), calls=%async_computation.2 | async-start | bytes 4194304 | tf_op jit(solution)/shard_map/all_to_all | solution.py:106
  145.6 50.2 %copy-start.8 = (bf16[128,512]{1,0:T(8,128)(2,1)S(1)}, bf16[128,512]{1,0:T(8,128)(2,1)}, u32[]{:S(2)}) copy-start(bf16[128,512]{1,0:T(8,128)(2,1)} %param.16) | copy-start | bytes 393220
  145.6 50.2 %copy-start.37 = (f32[512]{0:T(512)S(1)}, f32[512]{0:T(512)}, u32[]{:S(2)}) copy-start(f32[512]{0:T(512)} %param.18) | copy-start | bytes 6148
  145.6 119.1 %reduce-scatter.2.cloned.1.call-start = ((), (), s32[]{:S(2)}) async-start(), calls=%async_computation.7 | async-start | bytes 2359296 | tf_op jit(solution)/shard_map/reduce_scatter | solution.py:124
  195.8 2.2 copy-start.9
  195.8 3.5 %copy-start.7 = (bf16[512,512]{1,0:T(8,128)(2,1)S(1)}, bf16[512,512]{1,0:T(8,128)(2,1)}, u32[]{:S(2)}) copy-start(bf16[512,512]{1,0:T(8,128)(2,1)} %copy-done.6) | copy-start | bytes 1572868
  199.3 4.4 %copy-start.42 = (bf16[8,64,2048]{2,1,0:T(8,128)(2,1)S(1)}, bf16[8,64,2048]{2,1,0:T(8,128)(2,1)}, u32[]{:S(2)}) copy-start(bf16[8,64,2048]{2,1,0:T(8,128)(2,1)} %all-gather.3.cloned.1.call-done) | copy-start | bytes 6291460
  199.3 4.4 %copy-start.43 = (f32[512,512]{1,0:T(8,128)S(1)}, f32[512,512]{1,0:T(8,128)}, u32[]{:S(2)}) copy-start(f32[512,512]{1,0:T(8,128)} %fusion.7) | copy-start | bytes 3145732
  199.3 4.4 %copy-start.44 = (f32[512,512]{1,0:T(8,128)S(1)}, f32[512,512]{1,0:T(8,128)}, u32[]{:S(2)}) copy-start(f32[512,512]{1,0:T(8,128)} %fusion.10) | copy-start | bytes 3145732
  203.7 2.7 copy-start.38
  203.7 2.7 copy-start.40
  206.4 10.0 %copy-start.5 = (bf16[512,512]{1,0:T(8,128)(2,1)S(1)}, bf16[512,512]{1,0:T(8,128)(2,1)}, u32[]{:S(2)}) copy-start(bf16[512,512]{1,0:T(8,128)(2,1)} %copy-done.4) | copy-start | bytes 1572868
  214.9 6.8 %copy-start.10 = (f32[1,512]{1,0:T(1,128)S(1)}, f32[1,512]{1,0:T(1,128)}, u32[]{:S(2)}) copy-start(f32[1,512]{1,0:T(1,128)} %get-tuple-element.34) | copy-start | bytes 6148
  214.9 6.8 %copy-start.11 = (f32[1,512]{1,0:T(1,128)S(1)}, f32[1,512]{1,0:T(1,128)}, u32[]{:S(2)}) copy-start(f32[1,512]{1,0:T(1,128)} %get-tuple-element.35) | copy-start | bytes 6148
  214.9 6.8 %copy-start.12 = (f32[1,512]{1,0:T(1,128)S(1)}, f32[1,512]{1,0:T(1,128)}, u32[]{:S(2)}) copy-start(f32[1,512]{1,0:T(1,128)} %get-tuple-element.36) | copy-start | bytes 6148
  214.9 6.8 %copy-start.13 = (f32[1,512]{1,0:T(1,128)S(1)}, f32[1,512]{1,0:T(1,128)}, u32[]{:S(2)}) copy-start(f32[1,512]{1,0:T(1,128)} %get-tuple-element.37) | copy-start | bytes 6148
  214.9 6.8 %copy-start.14 = (f32[1,512]{1,0:T(1,128)S(1)}, f32[1,512]{1,0:T(1,128)}, u32[]{:S(2)}) copy-start(f32[1,512]{1,0:T(1,128)} %get-tuple-element.38) | copy-start | bytes 6148
  214.9 6.8 %copy-start.15 = (f32[1,512]{1,0:T(1,128)S(1)}, f32[1,512]{1,0:T(1,128)}, u32[]{:S(2)}) copy-start(f32[1,512]{1,0:T(1,128)} %get-tuple-element.39) | copy-start | bytes 6148
  214.9 6.8 %copy-start.16 = (f32[1,512]{1,0:T(1,128)S(1)}, f32[1,512]{1,0:T(1,128)}, u32[]{:S(2)}) copy-start(f32[1,512]{1,0:T(1,128)} %get-tuple-element.40) | copy-start | bytes 6148
  215.0 6.8 %copy-start.17 = (f32[1,512]{1,0:T(1,128)S(1)}, f32[1,512]{1,0:T(1,128)}, u32[]{:S(2)}) copy-start(f32[1,512]{1,0:T(1,128)} %get-tuple-element.41) | copy-start | bytes 6148
  215.0 6.8 %copy-start.18 = (f32[1,512]{1,0:T(1,128)S(1)}, f32[1,512]{1,0:T(1,128)}, u32[]{:S(2)}) copy-start(f32[1,512]{1,0:T(1,128)} %get-tuple-element.11) | copy-start | bytes 6148
  215.0 6.8 %copy-start.19 = (f32[1,512]{1,0:T(1,128)S(1)}, f32[1,512]{1,0:T(1,128)}, u32[]{:S(2)}) copy-start(f32[1,512]{1,0:T(1,128)} %get-tuple-element.12) | copy-start | bytes 6148
  215.0 6.8 %copy-start.20 = (f32[1,512]{1,0:T(1,128)S(1)}, f32[1,512]{1,0:T(1,128)}, u32[]{:S(2)}) copy-start(f32[1,512]{1,0:T(1,128)} %get-tuple-element.13) | copy-start | bytes 6148
  215.0 6.8 %copy-start.21 = (f32[1,512]{1,0:T(1,128)S(1)}, f32[1,512]{1,0:T(1,128)}, u32[]{:S(2)}) copy-start(f32[1,512]{1,0:T(1,128)} %get-tuple-element.14) | copy-start | bytes 6148
  215.0 6.8 %copy-start.22 = (f32[1,512]{1,0:T(1,128)S(1)}, f32[1,512]{1,0:T(1,128)}, u32[]{:S(2)}) copy-start(f32[1,512]{1,0:T(1,128)} %get-tuple-element.15) | copy-start | bytes 6148
  215.0 6.8 %copy-start.23 = (f32[1,512]{1,0:T(1,128)S(1)}, f32[1,512]{1,0:T(1,128)}, u32[]{:S(2)}) copy-start(f32[1,512]{1,0:T(1,128)} %get-tuple-element.16) | copy-start | bytes 6148
  215.0 6.8 %copy-start.24 = (f32[1,512]{1,0:T(1,128)S(1)}, f32[1,512]{1,0:T(1,128)}, u32[]{:S(2)}) copy-start(f32[1,512]{1,0:T(1,128)} %get-tuple-element.17) | copy-start | bytes 6148
  215.0 6.8 %copy-start.25 = (f32[1,512]{1,0:T(1,128)S(1)}, f32[1,512]{1,0:T(1,128)}, u32[]{:S(2)}) copy-start(f32[1,512]{1,0:T(1,128)} %get-tuple-element.18) | copy-start | bytes 6148
  215.0 6.8 %copy-start.26 = (f32[1,512]{1,0:T(1,128)S(1)}, f32[1,512]{1,0:T(1,128)}, u32[]{:S(2)}) copy-start(f32[1,512]{1,0:T(1,128)} %get-tuple-element.19) | copy-start | bytes 6148
  215.1 6.8 %copy-start.27 = (f32[1,512]{1,0:T(1,128)S(1)}, f32[1,512]{1,0:T(1,128)}, u32[]{:S(2)}) copy-start(f32[1,512]{1,0:T(1,128)} %get-tuple-element.20) | copy-start | bytes 6148
  215.1 6.8 %copy-start.28 = (f32[1,512]{1,0:T(1,128)S(1)}, f32[1,512]{1,0:T(1,128)}, u32[]{:S(2)}) copy-start(f32[1,512]{1,0:T(1,128)} %get-tuple-element.21) | copy-start | bytes 6148
  215.1 6.8 %copy-start.29 = (f32[1,512]{1,0:T(1,128)S(1)}, f32[1,512]{1,0:T(1,128)}, u32[]{:S(2)}) copy-start(f32[1,512]{1,0:T(1,128)} %get-tuple-element.22) | copy-start | bytes 6148
  215.1 6.8 %copy-start.30 = (f32[1,512]{1,0:T(1,128)S(1)}, f32[1,512]{1,0:T(1,128)}, u32[]{:S(2)}) copy-start(f32[1,512]{1,0:T(1,128)} %get-tuple-element.23) | copy-start | bytes 6148
  215.1 6.8 %copy-start.31 = (f32[1,512]{1,0:T(1,128)S(1)}, f32[1,512]{1,0:T(1,128)}, u32[]{:S(2)}) copy-start(f32[1,512]{1,0:T(1,128)} %get-tuple-element.24) | copy-start | bytes 6148
  215.1 6.8 %copy-start.32 = (f32[1,512]{1,0:T(1,128)S(1)}, f32[1,512]{1,0:T(1,128)}, u32[]{:S(2)}) copy-start(f32[1,512]{1,0:T(1,128)} %get-tuple-element.25) | copy-start | bytes 6148
  215.1 6.8 %copy-start.33 = (f32[1,512]{1,0:T(1,128)S(1)}, f32[1,512]{1,0:T(1,128)}, u32[]{:S(2)}) copy-start(f32[1,512]{1,0:T(1,128)} %get-tuple-element.26) | copy-start | bytes 6148
  215.1 6.8 %copy-start.34 = (f32[1,512]{1,0:T(1,128)S(1)}, f32[1,512]{1,0:T(1,128)}, u32[]{:S(2)}) copy-start(f32[1,512]{1,0:T(1,128)} %get-tuple-element.27) | copy-start | bytes 6148
  215.1 6.8 %copy-start.35 = (f32[1,512]{1,0:T(1,128)S(1)}, f32[1,512]{1,0:T(1,128)}, u32[]{:S(2)}) copy-start(f32[1,512]{1,0:T(1,128)} %get-tuple-element.28) | copy-start | bytes 6148
  215.1 6.8 %copy-start.36 = (f32[1,512]{1,0:T(1,128)S(1)}, f32[1,512]{1,0:T(1,128)}, u32[]{:S(2)}) copy-start(f32[1,512]{1,0:T(1,128)} %get-tuple-element.29) | copy-start | bytes 6148
  215.2 6.5 %collective-permute-start = (f32[30,512]{1,0:T(8,128)S(1)}, f32[30,512]{1,0:T(8,128)S(1)}, u32[]{:S(2)}, u32[]{:S(2)}) collective-permute-start(f32[30,512]{1,0:T(8,128)S(1)} %slice.257), channel_id=1, source_target_pairs={{4,0},{8,4},{12,8},{16,12},{20,16},{24,20},{28,24},{5,1},{9,5},{13... | collective-permute-start | bytes 184328 | tf_op jit(solution)/shard_map/ppermute | solution.py:10
  (3 other events, 4.7 us)
Sparse Core Ops, SparseCore 0:
  33.8 21.5 all-gather.4
  57.0 22.5 all-gather.2
  88.7 51.3 all-reduce.2
  198.1 66.5 reduce-scatter.1
where the time goes:
time: 274 us; the launch traced here: 273 us
  waiting for transfers between devices  163 us (59%)
  blocking collectives  45.5 us (17%)
  matrix products  33.1 us (12%)
  between operations  14.5 us (5%)
  starting transfers between devices  6.96 us (3%)
  other arithmetic  6.52 us (2%)
  local copies, waits for them, and re-layouts  3.94 us (1%)
    psum x1, waiting for transfers between devices, shards(): summed = lax.psum(partial_value.astype(jnp.bfloat16), 'tp')  51.5 us
    all_to_all x1, waiting for transfers between devices, shards(): lax.all_to_all(summed.reshape(experts, capacity, model_width), 'sp', spli...  47.7 us
    reduce_scatter x1, waiting for transfers between devices, shards(): lax.psum_scatter(lax.dot_general(mixer_grad, act_conv, contract_first, pr...  40.9 us
    all_to_all x1, blocking collectives, shards(): lax.all_to_all(sent_rows, 'sp', split_axis=0, concat_axis=0, tiled=True)  21.7 us
    all_gather x1, waiting for transfers between devices, shards(): lax.all_gather(shared_rows[1], 'tp', axis=1, tiled=True)  17.9 us
    all_to_all x1, blocking collectives, shards(): lax.all_to_all(sent_grad, 'sp', split_axis=0, concat_axis=0, tiled=True)  17.6 us
    psum x1, blocking collectives, shards(): lax.psum((jnp.sum(norm_output_gradient, axis=1), jnp.sum(norm_output_grad...  6.16 us
    all_to_all x1, starting transfers between devices, shards(): lax.all_to_all(summed.reshape(experts, capacity, model_width), 'sp', spli...  5.51 us
  transfers between devices with their start and end apart: 6, of which 6 were waited for; matrix products, arithmetic and copies ran while one was open for 9% of the time, Pallas kernels for 0%

commit v1 on v0

--- a/solution.py
+++ b/solution.py
@@ -66,7 +66,7 @@
     )
     routed_rows, routed_grad = (
         lax.all_gather(shared_rows[0], "tp", axis=1, tiled=True),
-        lax.all_gather(shared_rows[1], "tp", axis=1, tiled=True),
+        jnp.concatenate(lax.all_gather(shared_rows[1], "tp"), axis=1),
     )
     full_table, unused_weight = route_table(
         expert_ids, route_weight, 0, capacity, capacity, experts

time: 274 us -> 277 us (1.011)
  matrix products: 33.1 us -> 28.5 us
  local copies, waits for them, and re-layouts: 3.94 us -> 8.19 us
  waiting for transfers between devices: 163 us -> 166 us
    all_gather x1, waiting for transfers between devices: 3.5 us -> 21 us  [shards(): lax.all_gather(shared_rows[0], 'tp', axis=1, tiled=True)]
    all_gather x1, waiting for transfers between devices: 17.9 us -> 3.68 us  [shards(): lax.all_gather(shared_rows[1], 'tp')]
    all_to_all x1, blocking collectives: 17.6 us -> 21.7 us  [shards(): lax.all_to_all(sent_grad, 'sp', split_axis=0, concat_axis=0, tiled=True)]
    all_to_all x1, blocking collectives: 21.7 us -> 17.6 us  [shards(): lax.all_to_all(sent_rows, 'sp', split_axis=0, concat_axis=0, tiled=True)]
    reshape x0 -> x1, local copies, waits for them, and re-layouts: none -> 3.16 us  [shards(): jnp.concatenate(lax.all_gather(shared_rows[1], 'tp'), axis=1)]
  transfers between devices with their start and end apart: 6 -> 6, of which waited for: 6 -> 6; matrix products, arithmetic and copies ran while one was open for 9% -> 7% of each run, Pallas kernels for 0% -> 0%
where the time goes in v1:
time: 277 us
  waiting for transfers between devices  166 us (60%)
  blocking collectives  45.7 us (16%)
  matrix products  28.5 us (10%)
  between operations  14.5 us (5%)
  local copies, waits for them, and re-layouts  8.19 us (3%)
  other arithmetic  7.2 us (3%)
  starting transfers between devices  6.96 us (3%)
    psum x1, waiting for transfers between devices, shards(): summed = lax.psum(partial_value.astype(jnp.bfloat16), 'tp')  51.5 us
    all_to_all x1, waiting for transfers between devices, shards(): lax.all_to_all(summed.reshape(experts, capacity, model_width), 'sp', spli...  47.7 us
    reduce_scatter x1, waiting for transfers between devices, shards(): lax.psum_scatter(lax.dot_general(mixer_grad, act_conv, contract_first, pr...  41.1 us
    all_to_all x1, blocking collectives, shards(): lax.all_to_all(sent_grad, 'sp', split_axis=0, concat_axis=0, tiled=True)  21.7 us
    all_gather x1, waiting for transfers between devices, shards(): lax.all_gather(shared_rows[0], 'tp', axis=1, tiled=True)  21 us
    all_to_all x1, blocking collectives, shards(): lax.all_to_all(sent_rows, 'sp', split_axis=0, concat_axis=0, tiled=True)  17.6 us
    psum x1, blocking collectives, shards(): lax.psum((jnp.sum(norm_output_gradient, axis=1), jnp.sum(norm_output_grad...  6.34 us
  transfers between devices with their start and end apart: 6, of which 6 were waited for; matrix products, arithmetic and copies ran while one was open for 7% of the time, Pallas kernels for 0%

profile of v1, /device:TPU:0, one launch (start us, length us, event | category | flops | bytes accessed | tf_op | source)
XLA Modules:
  0.0 276.9 jit_solution(1488121317966146279)
XLA Ops:
  7.2 1.0 copy.44
  8.2 0.1 eq.63
  8.4 0.1 eq.59
  8.5 0.1 iota_add_fusion
  8.6 0.1 add.181
  8.7 0.6 reduce-window.6
  9.3 0.2 slice_reduce_fusion
  9.5 0.1 fusion.124
  9.6 0.1 reshape.97
  9.8 0.1 copy.46
  9.8 0.7 multiply_add_fusion
  10.5 0.1 compare_reduce_fusion.1
  10.6 0.9 fusion.120
  11.5 1.3 fusion.3
  12.8 21.7 %all_to_all.15 = bf16[8,16,2048]{2,1,0:T(8,128)(2,1)} all-to-all(bf16[8,16,2048]{2,1,0:T(8,128)(2,1)S(1)} %bitcast.92), channel_id=1, replica_groups=mesh['sp'=8,'tp'=4] {'sp'}, dimensions={0} | all-to-all | bytes 1048576 | tf_op jit(solution)/shard_map/all_to_all | solution.py:65
  34.6 0.3 convolution_convert_fusion.4
  34.9 17.6 %all_to_all.16 = bf16[8,16,2048]{2,1,0:T(8,128)(2,1)} all-to-all(bf16[8,16,2048]{2,1,0:T(8,128)(2,1)S(1)} %bitcast.93), channel_id=1, replica_groups=mesh['sp'=8,'tp'=4] {'sp'}, dimensions={0} | all-to-all | bytes 1048576 | tf_op jit(solution)/shard_map/all_to_all | solution.py:64
  52.6 3.7 %all-gather.6.cloned.1.call-done = bf16[32,16,2048]{2,1,0:T(8,128)(2,1)} async-done(((bf16[8,16,2048]{2,1,0:T(8,128)(2,1)}), bf16[32,16,2048]{2,1,0:T(8,128)(2,1)}) %all-gather.6.cloned.1.call-update) | async-done | bytes 2097168 | tf_op jit(solution)/shard_map/all_gather | solution.py:69
  56.3 3.2 %copy.47 = bf16[8,4,16,2048]{3,2,1,0:T(8,128)(2,1)} copy(bf16[8,4,16,2048]{3,2,0,1:T(8,128)(2,1)} %bitcast.91) | data formatting | bytes 4194304 | tf_op jit(solution)/shard_map/reshape | solution.py:69
  59.5 21.0 %all-gather.4.cloned.1.call-done = bf16[8,64,2048]{2,1,0:T(8,128)(2,1)} async-done(((bf16[8,16,2048]{2,1,0:T(8,128)(2,1)}), bf16[8,64,2048]{2,1,0:T(8,128)(2,1)}) %all-gather.4.cloned.1.call-update) | async-done | bytes 2097168 | tf_op jit(solution)/shard_map/all_gather | solution.py:68
  80.5 3.0 %fusion.7 = f32[512,512]{1,0:T(8,128)S(1)} fusion(bf16[512,2048]{1,0:T(8,128)(2,1)} %bitcast.125, bf16[1,2048,512]{2,1,0:T(8,128)(2,1)S(1)} %copy-done), kind=kOutput, calls=%fused_computation.44 | convolution fusion | flops 1073741824 | bytes 5242880 | tf_op jit(solution)/shard_map/dot_general | solution.py:81
  83.5 1.2 fusion.10
  84.8 0.7 copy-done.3
  85.5 1.0 copy-done.41
  86.5 1.7 multiply_convert_fusion.1
  88.2 1.3 fusion.5
  89.5 2.6 add_convert_fusion
  92.1 51.5 %all-reduce.3.cloned.1.call-done = bf16[8,64,2048]{2,1,0:T(8,128)(2,1)} async-done(((bf16[8,64,2048]{2,1,0:T(8,128)(2,1)}), bf16[8,64,2048]{2,1,0:T(8,128)(2,1)}) %all-reduce.3.cloned.1.call-update) | async-done | bytes 2097168 | tf_op jit(solution)/shard_map/psum | solution.py:105
  143.7 5.5 %all-to-all-start.2 = ((bf16[8,64,2048]{2,1,0:T(8,128)(2,1)}), bf16[8,64,2048]{2,1,0:T(8,128)(2,1)}, u32[]{:S(2)}, u32[]{:S(2)}) async-start(bf16[8,64,2048]{2,1,0:T(8,128)(2,1)} %all-reduce.3.cloned.1.call-done), calls=%async_computation.2 | async-start | bytes 4194304 | tf_op jit(solution)/shard_map/all_to_all | solution.py:106
  149.3 0.1 iota_add_fusion.1
  149.3 0.1 add.175
  149.4 0.1 compare_reduce_fusion
  149.6 47.7 %all-to-all-done.2 = bf16[8,64,2048]{2,1,0:T(8,128)(2,1)} async-done(((bf16[8,64,2048]{2,1,0:T(8,128)(2,1)}), bf16[8,64,2048]{2,1,0:T(8,128)(2,1)}, u32[]{:S(2)}, u32[]{:S(2)}) %all-to-all-start.2) | async-done | bytes 2097184 | tf_op jit(solution)/shard_map/all_to_all | solution.py:106
  197.3 2.1 fusion.4
  199.4 2.1 convolution_convert_fusion
  201.6 0.6 fusion.130
  202.2 0.7 fusion.129
  202.9 4.4 %fusion.1 = bf16[1,2048,512]{2,1,0:T(8,128)(2,1)} fusion(bf16[512,2048]{1,0:T(8,128)(2,1)} %bitcast.126, bf16[512,512]{1,0:T(8,128)(2,1)S(1)} %copy-done.8), kind=kOutput, calls=%fused_computation.35 | convolution fusion | flops 1074790400 | bytes 4718592 | tf_op jit(solution)/shard_map/dot_general | solution.py:99
  207.3 2.7 fusion.2
  210.0 1.6 fusion.128
  211.6 6.3 %all-reduce = (f32[128]{0:T(128)S(1)}, f32[128]{0:T(128)S(1)}) all-reduce(f32[128]{0:T(128)} %get-tuple-element.6, f32[128]{0:T(128)} %get-tuple-element.5), channel_id=1, replica_groups=mesh['sp'=8,'tp'=4] {'tp'}, use_global_device_ids=true, to_apply=%region_10.11 | all-reduce | flops 256 | bytes 2048 | tf_op jit(solution)/shard_map/psum | solution.py:141
  218.0 0.8 fusion.27
  219.0 1.3 collective-permute-start
  220.3 4.3 %fusion = bf16[1,2048,512]{2,1,0:T(8,128)(2,1)} fusion(bf16[512,2048]{1,0:T(8,128)(2,1)} %bitcast.127, bf16[512,512]{1,0:T(8,128)(2,1)S(1)} %copy-done.6), kind=kOutput, calls=%fused_computation.34 | convolution fusion | flops 1074790400 | bytes 4718592 | tf_op jit(solution)/shard_map/dot_general | solution.py:96
  224.6 0.7 collective-permute-done
  225.5 2.0 fusion.32
  227.5 41.1 %reduce-scatter.2.cloned.1.call-done = bf16[256,512]{1,0:T(8,128)(2,1)} async-done(((bf16[2048,512]{1,0:T(8,128)(2,1)}), bf16[256,512]{1,0:T(8,128)(2,1)}) %reduce-scatter.2.cloned.1.call-update) | async-done | bytes 262160 | tf_op jit(solution)/shard_map/reduce_scatter | solution.py:124
  268.6 1.8 convert_element_type.72
  (109 shorter events, 0.5 us)
Async XLA Ops:
  7.2 73.3 %copy-start = (bf16[1,2048,512]{2,1,0:T(8,128)(2,1)S(1)}, bf16[1,2048,512]{2,1,0:T(8,128)(2,1)}, u32[]{:S(2)}) copy-start(bf16[1,2048,512]{2,1,0:T(8,128)(2,1)} %param.21) | copy-start | bytes 6291460
  7.2 27.4 %copy-start.9 = (bf16[128,2048]{1,0:T(8,128)(2,1)S(1)}, bf16[128,2048]{1,0:T(8,128)(2,1)}, u32[]{:S(2)}) copy-start(bf16[128,2048]{1,0:T(8,128)(2,1)} %param.13) | copy-start | bytes 1572868
  7.2 49.1 %all-gather.6.cloned.1.call-start = ((), (), s32[]{:S(2)}) async-start(), calls=%async_computation.7 | async-start | bytes 2621440 | tf_op jit(solution)/shard_map/all_gather | solution.py:69
  34.6 45.9 %all-gather.4.cloned.1.call-start = ((), (), s32[]{:S(2)}) async-start(), calls=%async_computation.4 | async-start | bytes 2621440 | tf_op jit(solution)/shard_map/all_gather | solution.py:68
  52.6 91.1 %all-reduce.3.cloned.1.call-start = ((), (), s32[]{:S(2)}) async-start(), calls=%async_computation.5 | async-start | bytes 4194304 | tf_op jit(solution)/shard_map/psum | solution.py:105
  80.5 3.0 %copy-start.1 = (bf16[1,2048,512]{2,1,0:T(8,128)(2,1)S(1)}, bf16[1,2048,512]{2,1,0:T(8,128)(2,1)}, u32[]{:S(2)}) copy-start(bf16[1,2048,512]{2,1,0:T(8,128)(2,1)} %param.22) | copy-start | bytes 6291460
  80.5 3.0 %copy-start.43 = (bf16[8,64,2048]{2,1,0:T(8,128)(2,1)S(1)}, bf16[8,64,2048]{2,1,0:T(8,128)(2,1)}, u32[]{:S(2)}) copy-start(bf16[8,64,2048]{2,1,0:T(8,128)(2,1)} %all-gather.4.cloned.1.call-done) | copy-start | bytes 6291460
  83.5 3.0 %copy-start.41 = (bf16[1,512,2048]{2,1,0:T(8,128)(2,1)S(1)}, bf16[1,512,2048]{2,1,0:T(8,128)(2,1)}, u32[]{:S(2)}) copy-start(bf16[1,512,2048]{2,1,0:T(8,128)(2,1)} %param.23) | copy-start | bytes 6291460
  84.8 3.4 %copy-start.46 = (f32[512,512]{1,0:T(8,128)}, f32[512,512]{1,0:T(8,128)S(1)}, u32[]{:S(2)}) copy-start(f32[512,512]{1,0:T(8,128)S(1)} %fusion.10) | copy-start | bytes 3145732
  92.1 105.2 %copy-start.2 = (bf16[128,2048]{1,0:T(8,128)(2,1)S(1)}, bf16[128,2048]{1,0:T(8,128)(2,1)}, u32[]{:S(2)}) copy-start(bf16[128,2048]{1,0:T(8,128)(2,1)} %param.12) | copy-start | bytes 1572868
  143.7 53.6 %all-to-all-start.2 = ((bf16[8,64,2048]{2,1,0:T(8,128)(2,1)}), bf16[8,64,2048]{2,1,0:T(8,128)(2,1)}, u32[]{:S(2)}, u32[]{:S(2)}) async-start(bf16[8,64,2048]{2,1,0:T(8,128)(2,1)} %all-reduce.3.cloned.1.call-done), calls=%async_computation.2 | async-start | bytes 4194304 | tf_op jit(solution)/shard_map/all_to_all | solution.py:106
  149.2 50.2 %copy-start.10 = (bf16[128,512]{1,0:T(8,128)(2,1)S(1)}, bf16[128,512]{1,0:T(8,128)(2,1)}, u32[]{:S(2)}) copy-start(bf16[128,512]{1,0:T(8,128)(2,1)} %param.16) | copy-start | bytes 393220
  149.2 50.2 %copy-start.39 = (f32[512]{0:T(512)S(1)}, f32[512]{0:T(512)}, u32[]{:S(2)}) copy-start(f32[512]{0:T(512)} %param.18) | copy-start | bytes 6148
  149.2 119.4 %reduce-scatter.2.cloned.1.call-start = ((), (), s32[]{:S(2)}) async-start(), calls=%async_computation.6 | async-start | bytes 2359296 | tf_op jit(solution)/shard_map/reduce_scatter | solution.py:124
  199.4 3.5 %copy-start.8 = (bf16[512,512]{1,0:T(8,128)(2,1)S(1)}, bf16[512,512]{1,0:T(8,128)(2,1)}, u32[]{:S(2)}) copy-start(bf16[512,512]{1,0:T(8,128)(2,1)} %copy-done.7) | copy-start | bytes 1572868
  202.9 4.4 %copy-start.4 = (bf16[8,4,16,2048]{3,2,1,0:T(8,128)(2,1)S(1)}, bf16[8,4,16,2048]{3,2,1,0:T(8,128)(2,1)}, u32[]{:S(2)}) copy-start(bf16[8,4,16,2048]{3,2,1,0:T(8,128)(2,1)} %copy.47) | copy-start | bytes 6291460
  202.9 4.4 %copy-start.45 = (f32[512,512]{1,0:T(8,128)S(1)}, f32[512,512]{1,0:T(8,128)}, u32[]{:S(2)}) copy-start(f32[512,512]{1,0:T(8,128)} %copy-done.44) | copy-start | bytes 3145732
  202.9 4.4 %copy-start.47 = (f32[512,512]{1,0:T(8,128)S(1)}, f32[512,512]{1,0:T(8,128)}, u32[]{:S(2)}) copy-start(f32[512,512]{1,0:T(8,128)} %copy-done.46) | copy-start | bytes 3145732
  207.3 2.8 %copy-start.40 = (f32[512]{0:T(512)S(1)}, f32[512]{0:T(512)}, u32[]{:S(2)}) copy-start(f32[512]{0:T(512)} %param.18) | copy-start | bytes 6148
  210.0 10.3 %copy-start.6 = (bf16[512,512]{1,0:T(8,128)(2,1)S(1)}, bf16[512,512]{1,0:T(8,128)(2,1)}, u32[]{:S(2)}) copy-start(bf16[512,512]{1,0:T(8,128)(2,1)} %copy-done.5) | copy-start | bytes 1572868
  218.7 6.5 %copy-start.12 = (f32[1,512]{1,0:T(1,128)S(1)}, f32[1,512]{1,0:T(1,128)}, u32[]{:S(2)}) copy-start(f32[1,512]{1,0:T(1,128)} %get-tuple-element.34) | copy-start | bytes 6148
  218.8 6.5 %copy-start.13 = (f32[1,512]{1,0:T(1,128)S(1)}, f32[1,512]{1,0:T(1,128)}, u32[]{:S(2)}) copy-start(f32[1,512]{1,0:T(1,128)} %get-tuple-element.35) | copy-start | bytes 6148
  218.8 6.5 %copy-start.14 = (f32[1,512]{1,0:T(1,128)S(1)}, f32[1,512]{1,0:T(1,128)}, u32[]{:S(2)}) copy-start(f32[1,512]{1,0:T(1,128)} %get-tuple-element.36) | copy-start | bytes 6148
  218.8 6.5 %copy-start.15 = (f32[1,512]{1,0:T(1,128)S(1)}, f32[1,512]{1,0:T(1,128)}, u32[]{:S(2)}) copy-start(f32[1,512]{1,0:T(1,128)} %get-tuple-element.37) | copy-start | bytes 6148
  218.8 6.5 %copy-start.16 = (f32[1,512]{1,0:T(1,128)S(1)}, f32[1,512]{1,0:T(1,128)}, u32[]{:S(2)}) copy-start(f32[1,512]{1,0:T(1,128)} %get-tuple-element.38) | copy-start | bytes 6148
  218.8 6.5 %copy-start.17 = (f32[1,512]{1,0:T(1,128)S(1)}, f32[1,512]{1,0:T(1,128)}, u32[]{:S(2)}) copy-start(f32[1,512]{1,0:T(1,128)} %get-tuple-element.39) | copy-start | bytes 6148
  218.8 6.5 %copy-start.18 = (f32[1,512]{1,0:T(1,128)S(1)}, f32[1,512]{1,0:T(1,128)}, u32[]{:S(2)}) copy-start(f32[1,512]{1,0:T(1,128)} %get-tuple-element.40) | copy-start | bytes 6148
  218.8 6.5 %copy-start.19 = (f32[1,512]{1,0:T(1,128)S(1)}, f32[1,512]{1,0:T(1,128)}, u32[]{:S(2)}) copy-start(f32[1,512]{1,0:T(1,128)} %get-tuple-element.41) | copy-start | bytes 6148
  218.8 6.5 %copy-start.20 = (f32[1,512]{1,0:T(1,128)S(1)}, f32[1,512]{1,0:T(1,128)}, u32[]{:S(2)}) copy-start(f32[1,512]{1,0:T(1,128)} %get-tuple-element.11) | copy-start | bytes 6148
  218.8 6.5 %copy-start.21 = (f32[1,512]{1,0:T(1,128)S(1)}, f32[1,512]{1,0:T(1,128)}, u32[]{:S(2)}) copy-start(f32[1,512]{1,0:T(1,128)} %get-tuple-element.12) | copy-start | bytes 6148
  218.8 6.5 %copy-start.22 = (f32[1,512]{1,0:T(1,128)S(1)}, f32[1,512]{1,0:T(1,128)}, u32[]{:S(2)}) copy-start(f32[1,512]{1,0:T(1,128)} %get-tuple-element.13) | copy-start | bytes 6148
  218.9 6.5 %copy-start.23 = (f32[1,512]{1,0:T(1,128)S(1)}, f32[1,512]{1,0:T(1,128)}, u32[]{:S(2)}) copy-start(f32[1,512]{1,0:T(1,128)} %get-tuple-element.14) | copy-start | bytes 6148
  218.9 6.5 %copy-start.24 = (f32[1,512]{1,0:T(1,128)S(1)}, f32[1,512]{1,0:T(1,128)}, u32[]{:S(2)}) copy-start(f32[1,512]{1,0:T(1,128)} %get-tuple-element.15) | copy-start | bytes 6148
  218.9 6.5 %copy-start.25 = (f32[1,512]{1,0:T(1,128)S(1)}, f32[1,512]{1,0:T(1,128)}, u32[]{:S(2)}) copy-start(f32[1,512]{1,0:T(1,128)} %get-tuple-element.16) | copy-start | bytes 6148
  218.9 6.5 %copy-start.26 = (f32[1,512]{1,0:T(1,128)S(1)}, f32[1,512]{1,0:T(1,128)}, u32[]{:S(2)}) copy-start(f32[1,512]{1,0:T(1,128)} %get-tuple-element.17) | copy-start | bytes 6148
  218.9 6.5 %copy-start.27 = (f32[1,512]{1,0:T(1,128)S(1)}, f32[1,512]{1,0:T(1,128)}, u32[]{:S(2)}) copy-start(f32[1,512]{1,0:T(1,128)} %get-tuple-element.18) | copy-start | bytes 6148
  218.9 6.5 %copy-start.28 = (f32[1,512]{1,0:T(1,128)S(1)}, f32[1,512]{1,0:T(1,128)}, u32[]{:S(2)}) copy-start(f32[1,512]{1,0:T(1,128)} %get-tuple-element.19) | copy-start | bytes 6148
  218.9 6.5 %copy-start.29 = (f32[1,512]{1,0:T(1,128)S(1)}, f32[1,512]{1,0:T(1,128)}, u32[]{:S(2)}) copy-start(f32[1,512]{1,0:T(1,128)} %get-tuple-element.20) | copy-start | bytes 6148
  218.9 6.5 %copy-start.30 = (f32[1,512]{1,0:T(1,128)S(1)}, f32[1,512]{1,0:T(1,128)}, u32[]{:S(2)}) copy-start(f32[1,512]{1,0:T(1,128)} %get-tuple-element.21) | copy-start | bytes 6148
  218.9 6.5 %copy-start.31 = (f32[1,512]{1,0:T(1,128)S(1)}, f32[1,512]{1,0:T(1,128)}, u32[]{:S(2)}) copy-start(f32[1,512]{1,0:T(1,128)} %get-tuple-element.22) | copy-start | bytes 6148
  218.9 6.5 %copy-start.32 = (f32[1,512]{1,0:T(1,128)S(1)}, f32[1,512]{1,0:T(1,128)}, u32[]{:S(2)}) copy-start(f32[1,512]{1,0:T(1,128)} %get-tuple-element.23) | copy-start | bytes 6148
  219.0 6.5 %copy-start.33 = (f32[1,512]{1,0:T(1,128)S(1)}, f32[1,512]{1,0:T(1,128)}, u32[]{:S(2)}) copy-start(f32[1,512]{1,0:T(1,128)} %get-tuple-element.24) | copy-start | bytes 6148
  219.0 6.5 %copy-start.34 = (f32[1,512]{1,0:T(1,128)S(1)}, f32[1,512]{1,0:T(1,128)}, u32[]{:S(2)}) copy-start(f32[1,512]{1,0:T(1,128)} %get-tuple-element.25) | copy-start | bytes 6148
  219.0 6.5 %copy-start.35 = (f32[1,512]{1,0:T(1,128)S(1)}, f32[1,512]{1,0:T(1,128)}, u32[]{:S(2)}) copy-start(f32[1,512]{1,0:T(1,128)} %get-tuple-element.26) | copy-start | bytes 6148
  219.0 6.5 %copy-start.36 = (f32[1,512]{1,0:T(1,128)S(1)}, f32[1,512]{1,0:T(1,128)}, u32[]{:S(2)}) copy-start(f32[1,512]{1,0:T(1,128)} %get-tuple-element.27) | copy-start | bytes 6148
  219.0 6.5 %copy-start.37 = (f32[1,512]{1,0:T(1,128)S(1)}, f32[1,512]{1,0:T(1,128)}, u32[]{:S(2)}) copy-start(f32[1,512]{1,0:T(1,128)} %get-tuple-element.28) | copy-start | bytes 6148
  219.0 6.5 %copy-start.38 = (f32[1,512]{1,0:T(1,128)S(1)}, f32[1,512]{1,0:T(1,128)}, u32[]{:S(2)}) copy-start(f32[1,512]{1,0:T(1,128)} %get-tuple-element.29) | copy-start | bytes 6148
  219.0 6.2 %collective-permute-start = (f32[30,512]{1,0:T(8,128)S(1)}, f32[30,512]{1,0:T(8,128)S(1)}, u32[]{:S(2)}, u32[]{:S(2)}) collective-permute-start(f32[30,512]{1,0:T(8,128)S(1)} %slice.257), channel_id=1, source_target_pairs={{4,0},{8,4},{12,8},{16,12},{20,16},{24,20},{28,24},{5,1},{9,5},{13... | collective-permute-start | bytes 184328 | tf_op jit(solution)/shard_map/ppermute | solution.py:10
  (6 other events, 10.9 us)
Sparse Core Ops, SparseCore 0:
  34.7 21.5 all-gather.5
  57.9 22.5 all-gather.3
  92.3 51.3 all-reduce.2
  201.7 66.8 reduce-scatter.1
